TPU v7x, 32 devices: a whole 2x2x4 slice. The times are simulated.
32 devices in a mesh: grp: 2 (over y), fs: 4 (over z), tp: 4 (over x, core).
Axes of the slice: x: 2, y: 2, z: 4, core: 2. Of those that a mesh axis runs over, the one named last changes fastest.
Arguments:
- stream: bfloat16 [8, 128, 2048], P(('grp', 'fs')), parts along dimension 0, may hold values from -6 to 6
- in_gain: float32 [2048], replicated, may hold values from 0.2 to 5
- value_weight: bfloat16 [2048, 1024], P('fs', 'tp'), may hold values from -0.125 to 0.125
- gate_weight: bfloat16 [2048, 1024], P('fs', 'tp'), may hold values from -0.125 to 0.125
- conv_kernel: bfloat16 [31, 1024], P(None, 'tp'), may hold values from -3.6 to 3.6
- conv_gain: float32 [1024], P('tp'), may hold values from 0.1 to 1.9
- conv_shift: float32 [1024], P('tp'), may hold values from -3 to 3
- out_weight: bfloat16 [1024, 2048], P('tp', 'fs'), may hold values from -0.1875 to 0.1875
- norm_gain: float32 [2048], replicated, may hold values from 0.2 to 5
- up_weight: bfloat16 [2048, 8192], P('fs', 'tp'), may hold values from -0.125 to 0.125
- down_weight: bfloat16 [8192, 2048], P('tp', 'fs'), may hold values from -0.0625 to 0.0625
- out_gain: float32 [2048], P('tp'), may hold values from 0.1 to 1.9
Outputs:
- result: bfloat16 [8, 128, 2048], P(('grp', 'fs'), None, 'tp'), parts along dimension 0
There are 2 independent parts, one for each index of `grp`. A program takes and returns all parts, laid end to end along the dimension named above; an argument that names none is the same for every part. Nothing has to cross between parts.
All inputs are finite; a program needn't handle non-finite values.
Results may differ from a plain program's by a relative error of at most 0.02.
Values may be sent and summed in bfloat16 or wider, within the bound.
A program may use at most 64 MiB of HBM per device.

v0:
```python
import jax
import jax.numpy as jnp
from jax import lax
from jax.sharding import PartitionSpec as P

KW = 31
norm_epsilon = 1e-05
residual_scale = 2.0**0.25


def norm_rows(values, gain_vector):
    row_mean = jnp.mean(values, axis=-1, keepdims=True)
    row_var = jnp.mean(jnp.square(values - row_mean), axis=-1, keepdims=True)
    return (values - row_mean) * lax.rsqrt(row_var + norm_epsilon) * gain_vector


def norm_shares(summed, stat_sums, full_width, gain_vector):
    row_mean = stat_sums[0] / full_width
    row_var = stat_sums[1] / full_width - row_mean * row_mean
    return (summed - row_mean[:, None]) * lax.rsqrt(row_var + norm_epsilon)[:, None] * gain_vector


def row_sums(summed):
    return (jnp.sum(summed, axis=1), jnp.sum(summed * summed, axis=1))


def contract(left, turned):
    return lax.dot_general(
        left, turned, (((1,), (1,)), ((), ())), preferred_element_type=jnp.float32
    )


def shards(
    stream,
    in_gain,
    value_weight,
    gate_weight,
    conv_kernel,
    conv_gain,
    conv_shift,
    out_weight,
    norm_gain,
    up_weight,
    down_weight,
    out_gain,
):
    seq_count, seq_length, model_width = stream.shape
    token_count = seq_count * seq_length
    tp_count = lax.axis_size("tp")
    slice_width = model_width // tp_count
    tp_index = lax.axis_index("tp")
    out_turned_shard = out_weight.T
    down_turned_shard = down_weight.T
    value_whole, gate_whole, out_turned, up_whole, down_turned = (
        lax.all_gather(value_weight, "fs", axis=0, tiled=True),
        lax.all_gather(gate_weight, "fs", axis=0, tiled=True),
        lax.all_gather(out_turned_shard, "fs", axis=0, tiled=True),
        lax.all_gather(up_weight, "fs", axis=0, tiled=True),
        lax.all_gather(down_turned_shard, "fs", axis=0, tiled=True),
    )
    normed = norm_rows(
        stream.reshape(token_count, model_width).astype(jnp.float32), in_gain
    ).astype(jnp.bfloat16)
    channels = value_weight.shape[1]
    values = jnp.dot(normed, value_whole, preferred_element_type=jnp.float32)
    gating = jnp.dot(normed, gate_whole, preferred_element_type=jnp.float32)
    gated = (values * jax.nn.sigmoid(gating)).astype(jnp.bfloat16)
    convolved = lax.conv_general_dilated(
        gated.reshape(seq_count, seq_length, channels),
        conv_kernel[:, None, :],
        window_strides=(1,),
        padding=[(KW - 1, 0)],
        dimension_numbers=("NWC", "WIO", "NWC"),
        feature_group_count=channels,
        preferred_element_type=jnp.float32,
    ).reshape(token_count, channels)
    conv_sums = lax.psum(row_sums(convolved), "tp")
    activated = jax.nn.silu(
        norm_shares(convolved, conv_sums, channels * tp_count, conv_gain) + conv_shift
    ).astype(jnp.bfloat16)
    partial_terms = contract(activated, out_turned)
    mixed = lax.psum_scatter(
        partial_terms.astype(jnp.bfloat16), "tp", scatter_dimension=1, tiled=True
    )
    normed_own = lax.dynamic_slice_in_dim(normed, tp_index * slice_width, slice_width, 1)
    gain_own = lax.dynamic_slice_in_dim(norm_gain, tp_index * slice_width, slice_width, 0)
    summed = residual_scale * normed_own.astype(jnp.float32) + mixed.astype(jnp.float32)
    mix_sums = lax.psum(row_sums(summed), "tp")
    settled_own = norm_shares(summed, mix_sums, model_width, gain_own).astype(jnp.bfloat16)
    settled_full = lax.all_gather(settled_own, "tp", axis=1, tiled=True)
    hidden = jnp.square(
        jax.nn.relu(jnp.dot(settled_full, up_whole, preferred_element_type=jnp.float32))
    ).astype(jnp.bfloat16)
    fed_terms = contract(hidden, down_turned)
    fed = lax.psum_scatter(fed_terms.astype(jnp.bfloat16), "tp", scatter_dimension=1, tiled=True)
    final_sum = residual_scale * settled_own.astype(jnp.float32) + fed.astype(jnp.float32)
    out_sums = lax.psum(row_sums(final_sum), "tp")
    result = norm_shares(final_sum, out_sums, model_width, out_gain).astype(jnp.bfloat16)
    return result.reshape(seq_count, seq_length, slice_width)


def solution(mesh):
    in_specs = (
        P(("grp", "fs"), None, None),
        P(),
        P("fs", "tp"),
        P("fs", "tp"),
        P(None, "tp"),
        P("tp"),
        P("tp"),
        P("tp", "fs"),
        P(),
        P("fs", "tp"),
        P("tp", "fs"),
        P("tp"),
    )
    out_specs = P(("grp", "fs"), None, "tp")
    return jax.shard_map(shards, mesh=mesh, in_specs=in_specs, out_specs=out_specs, check_vma=False)
```

profile of v0, /device:TPU:0, one launch (start us, length us, event | category | flops | bytes accessed | tf_op | source)
XLA Modules:
  0.0 465.8 jit_solution(17300026285777350739)
XLA Ops:
  6.5 0.7 all-gather.6.cloned.1.call-update
  7.3 0.7 all-gather.8.cloned.1.call-update
  8.1 0.7 all-gather.10.cloned.1.call-update
  8.7 0.0 reduce-scatter.3.cloned.1.call-start
  8.8 1.2 convert_reduce_fusion
  10.0 1.3 fusion.11
  11.3 1.4 fusion.13
  12.8 26.9 %all-gather.6.cloned.1.call-done = bf16[2048,256]{1,0:T(8,128)(2,1)} async-done(((bf16[512,256]{1,0:T(8,128)(2,1)}), bf16[2048,256]{1,0:T(8,128)(2,1)}) %all-gather.6.cloned.1.call-update) | async-done | bytes 1048592 | tf_op jit(solution)/shard_map/all_gather | solution.py:55
  39.6 1.5 fusion.33
  41.2 27.4 %all-gather.8.cloned.1.call-done = bf16[2048,256]{1,0:T(8,128)(2,1)} async-done(((bf16[512,256]{1,0:T(8,128)(2,1)}), bf16[2048,256]{1,0:T(8,128)(2,1)}) %all-gather.8.cloned.1.call-update) | async-done | bytes 1048592 | tf_op jit(solution)/shard_map/all_gather | solution.py:56
  68.6 1.5 fusion.7
  70.2 2.2 fusion.32
  72.3 0.1 fusion.21
  72.5 6.1 %all-reduce.2 = (f32[128]{0:T(128)S(1)}, f32[128]{0:T(128)S(1)}) all-reduce(f32[128]{0:T(128)S(1)} %fusion.21, f32[128]{0:T(128)S(1)} %get-tuple-element.21), channel_id=1, replica_groups=mesh['grp'=2,'fs'=4,'tp'=4] {'tp'}, use_global_device_ids=true, to_apply=%region_5.0 | all-reduce | flops 256 | bytes 2048 | tf_op jit(solution)/shard_map/psum | solution.py:77
  78.5 19.0 %all-gather.10.cloned.1.call-done = bf16[2048,256]{0,1:T(8,128)(2,1)} async-done(((bf16[512,256]{0,1:T(8,128)(2,1)}), bf16[2048,256]{0,1:T(8,128)(2,1)}) %all-gather.10.cloned.1.call-update) | async-done | bytes 1048592 | tf_op jit(solution)/shard_map/all_gather | solution.py:57
  97.6 2.4 convolution_convert_fusion.1
  100.0 0.0 all-gather.12.cloned.1.call-start
  100.1 0.5 all-gather.12.cloned.1.call-update
  100.6 0.5 all-gather.14.cloned.1.call-update
  101.2 0.8 dynamic_slice.7
  102.0 19.2 %reduce-scatter.3.cloned.1.call-done = bf16[128,512]{1,0:T(8,128)(2,1)} async-done(((bf16[128,2048]{1,0:T(8,128)(2,1)}), bf16[128,512]{1,0:T(8,128)(2,1)}) %reduce-scatter.3.cloned.1.call-update) | async-done | bytes 131088 | tf_op jit(solution)/shard_map/reduce_scatter | solution.py:82
  121.2 1.0 fusion.15
  122.2 5.8 %all-reduce.1 = (f32[128]{0:T(128)S(1)}, f32[128]{0:T(128)S(1)}) all-reduce(f32[128]{0:T(128)S(1)} %get-tuple-element.6, f32[128]{0:T(128)S(1)} %get-tuple-element.5), channel_id=1, replica_groups=mesh['grp'=2,'fs'=4,'tp'=4] {'tp'}, use_global_device_ids=true, to_apply=%region_10.11 | all-reduce | flops 256 | bytes 2048 | tf_op jit(solution)/shard_map/psum | solution.py:88
  128.0 1.0 multiply_convert_fusion.1
  129.0 6.9 %all_gather.21 = bf16[128,2048]{1,0:T(8,128)(2,1)S(1)} all-gather(bf16[128,512]{1,0:T(8,128)(2,1)S(1)} %multiply_convert_fusion.1), channel_id=1, replica_groups=mesh['grp'=2,'fs'=4,'tp'=4] {'tp'}, dimensions={1}, use_global_device_ids=true | all-gather | bytes 655360 | tf_op jit(solution)/shard_map/all_gather | solution.py:90
  135.9 136.3 %all-gather.12.cloned.1.call-done = bf16[2048,2048]{1,0:T(8,128)(2,1)} async-done(((bf16[512,2048]{1,0:T(8,128)(2,1)}), bf16[2048,2048]{1,0:T(8,128)(2,1)}) %all-gather.12.cloned.1.call-update) | async-done | bytes 8388624 | tf_op jit(solution)/shard_map/all_gather | solution.py:58
  272.2 149.3 %all-gather.14.cloned.1.call-done = bf16[2048,2048]{0,1:T(8,128)(2,1)} async-done(((bf16[512,2048]{0,1:T(8,128)(2,1)}), bf16[2048,2048]{0,1:T(8,128)(2,1)}) %all-gather.14.cloned.1.call-update) | async-done | bytes 8388624 | tf_op jit(solution)/shard_map/all_gather | solution.py:59
  421.5 8.9 %convolution_convert_fusion = bf16[128,2048]{1,0:T(8,128)(2,1)} fusion(bf16[2048,2048]{0,1:T(8,128)(2,1)} %all-gather.14.cloned.1.call-done, bf16[128,2048]{1,0:T(8,128)(2,1)S(1)} %all_gather.21, bf16[2048,2048]{1,0:T(8,128)(2,1)} %all-gather.12.cloned.1.call-done), kind=kOutput, calls=%fused_computation.2 | convolution fusion | flops 2148532224 | bytes 17825792 | tf_op jit(solution)/shard_map/dot_general | solution.py:28
  430.5 20.0 %reduce-scatter.5.cloned.1.call-done = bf16[128,512]{1,0:T(8,128)(2,1)} async-done(((bf16[128,2048]{1,0:T(8,128)(2,1)}), bf16[128,512]{1,0:T(8,128)(2,1)}) %reduce-scatter.5.cloned.1.call-update) | async-done | bytes 131088 | tf_op jit(solution)/shard_map/reduce_scatter | solution.py:95
  450.4 1.0 fusion.16
  451.5 5.8 %all-reduce = (f32[128]{0:T(128)S(1)}, f32[128]{0:T(128)S(1)}) all-reduce(f32[128]{0:T(128)S(1)} %get-tuple-element.8, f32[128]{0:T(128)S(1)} %get-tuple-element.7), channel_id=1, replica_groups=mesh['grp'=2,'fs'=4,'tp'=4] {'tp'}, use_global_device_ids=true, to_apply=%region_15.16 | all-reduce | flops 256 | bytes 2048 | tf_op jit(solution)/shard_map/psum | solution.py:97
  457.2 1.7 fusion.17
  (20 shorter events, 0.2 us)
Async XLA Ops:
  6.5 63.6 %copy-start = (bf16[31,256]{1,0:T(8,128)(2,1)S(1)}, bf16[31,256]{1,0:T(8,128)(2,1)}, u32[]{:S(2)}) copy-start(bf16[31,256]{1,0:T(8,128)(2,1)} %param.16) | copy-start | bytes 47620
  6.5 91.0 %copy-start.3 = (f32[256]{0:T(256)S(1)}, f32[256]{0:T(256)}, u32[]{:S(2)}) copy-start(f32[256]{0:T(256)} %param.17) | copy-start | bytes 3076
  6.5 91.0 %copy-start.2 = (f32[256]{0:T(256)S(1)}, f32[256]{0:T(256)}, u32[]{:S(2)}) copy-start(f32[256]{0:T(256)} %param.18) | copy-start | bytes 3076
  6.5 33.1 %all-gather.6.cloned.1.call-start = ((), (), s32[]{:S(2)}) async-start(), calls=%async_computation.2 | async-start | bytes 1310720 | tf_op jit(solution)/shard_map/all_gather | solution.py:55
  7.3 61.3 %all-gather.8.cloned.1.call-start = ((), (), s32[]{:S(2)}) async-start(), calls=%async_computation.3 | async-start | bytes 1310720 | tf_op jit(solution)/shard_map/all_gather | solution.py:56
  8.0 89.6 %all-gather.10.cloned.1.call-start = ((), (), s32[]{:S(2)}) async-start(), calls=%async_computation.4 | async-start | bytes 1310720 | tf_op jit(solution)/shard_map/all_gather | solution.py:57
  8.7 112.4 %reduce-scatter.3.cloned.1.call-start = ((), (), s32[]{:S(2)}) async-start(), calls=%async_computation.5 | async-start | bytes 655360 | tf_op jit(solution)/shard_map/reduce_scatter | solution.py:82
  100.0 172.2 %all-gather.12.cloned.1.call-start = ((), (), s32[]{:S(2)}) async-start(), calls=%async_computation.6 | async-start | bytes 10485760 | tf_op jit(solution)/shard_map/all_gather | solution.py:58
  100.6 320.9 %all-gather.14.cloned.1.call-start = ((), (), s32[]{:S(2)}) async-start(), calls=%async_computation.7 | async-start | bytes 10485760 | tf_op jit(solution)/shard_map/all_gather | solution.py:59
  101.2 349.2 %reduce-scatter.5.cloned.1.call-start = ((), (), s32[]{:S(2)}) async-start(), calls=%async_computation.8 | async-start | bytes 655360 | tf_op jit(solution)/shard_map/reduce_scatter | solution.py:95
  135.9 321.3 %copy-start.1 = (f32[512]{0:T(512)S(1)}, f32[512]{0:T(512)}, u32[]{:S(2)}) copy-start(f32[512]{0:T(512)} %param.23) | copy-start | bytes 6148
Sparse Core Ops, SparseCore 0:
  8.9 30.6 all-gather.5
  41.2 27.3 all-gather.7
  70.2 27.3 all-gather.9
  100.1 20.9 reduce-scatter.2
  122.6 149.6 all-gather.11
  273.7 147.7 all-gather.13
  430.6 19.7 reduce-scatter.4
where the time goes:
time: 466 us
  waiting for transfers between devices  401 us (86%)
  blocking collectives  24.5 us (5%)
  matrix products  16.6 us (4%)
  between operations  13.5 us (3%)
  other arithmetic  8.9 us (2%)
    all_gather x1, waiting for transfers between devices, shards(): lax.all_gather(down_turned_shard, 'fs', axis=0, tiled=True)  149 us
    all_gather x1, waiting for transfers between devices, shards(): lax.all_gather(up_weight, 'fs', axis=0, tiled=True)  136 us
    all_gather x1, waiting for transfers between devices, shards(): lax.all_gather(gate_weight, 'fs', axis=0, tiled=True)  27.4 us
    all_gather x1, waiting for transfers between devices, shards(): lax.all_gather(value_weight, 'fs', axis=0, tiled=True)  26.9 us
    reduce_scatter x1, waiting for transfers between devices, shards(): lax.psum_scatter(fed_terms.astype(jnp.bfloat16), 'tp', scatter_dimension=...  20 us
    reduce_scatter x1, waiting for transfers between devices, shards(): lax.psum_scatter(partial_terms.astype(jnp.bfloat16), 'tp', scatter_dimens...  19.2 us
    all_gather x1, waiting for transfers between devices, shards(): lax.all_gather(out_turned_shard, 'fs', axis=0, tiled=True)  19 us
    dot_general x2, matrix products, contract(): lax.dot_general(left, turned, (((1,), (1,)), ((), ())), preferred_element...  11.3 us
  transfers between devices with their start and end apart: 7, of which 7 were waited for; matrix products, arithmetic and copies ran while one was open for 3% of the time, Pallas kernels for 0%

commit v1 on v0

--- a/solution.py
+++ b/solution.py
@@ -6,6 +6,13 @@
 KW = 31
 norm_epsilon = 1e-05
 residual_scale = 2.0**0.25
+
+
+def drive_the_tasks(mine, pos_dim):
+    mine = jnp.moveaxis(mine, 0, pos_dim)
+    val = mine.shape
+    d_next = mine.reshape(*val[:pos_dim], val[pos_dim] * val[pos_dim + 1], *val[pos_dim + 2 :])
+    return d_next
 
 
 def norm_rows(values, gain_vector):
@@ -44,6 +51,22 @@
     down_weight,
     out_gain,
 ):
+
+    def _define_levels_all(packet, axis_id, at_axis):
+        wide_n = lax.axis_size(axis_id)
+        piece_out = range(wide_n)
+        clean = map(lambda rr: (rr, (rr + 1) % wide_n), piece_out)
+        buffer = list(clean)
+        leaves = [packet]
+        while len(leaves) < wide_n:
+            small = lax.ppermute(leaves[-1], axis_id, buffer)
+            leaves.append(small)
+        outcome_arr = lax.axis_index(axis_id)
+        res = jnp.stack(leaves)
+        leaves = res[(outcome_arr - jnp.arange(wide_n)) % wide_n]
+        p_next = drive_the_tasks(leaves, at_axis)
+        return p_next
+
     seq_count, seq_length, model_width = stream.shape
     token_count = seq_count * seq_length
     tp_count = lax.axis_size("tp")
@@ -52,7 +75,7 @@
     out_turned_shard = out_weight.T
     down_turned_shard = down_weight.T
     value_whole, gate_whole, out_turned, up_whole, down_turned = (
-        lax.all_gather(value_weight, "fs", axis=0, tiled=True),
+        _define_levels_all(value_weight, "fs", 0),
         lax.all_gather(gate_weight, "fs", axis=0, tiled=True),
         lax.all_gather(out_turned_shard, "fs", axis=0, tiled=True),
         lax.all_gather(up_weight, "fs", axis=0, tiled=True),

time: 466 us -> 447 us (0.959)
  waiting for transfers between devices: 401 us -> 377 us
    ppermute x0 -> x3, waiting for transfers between devices: none -> 35.2 us  [_define_levels_all(): small = lax.ppermute(leaves[-1], axis_id, buffer)]
    all_gather x1, waiting for transfers between devices: 27.4 us -> 0.02 us  [shards(): lax.all_gather(gate_weight, 'fs', axis=0, tiled=True)]
    all_gather x1 -> x0, waiting for transfers between devices: 26.9 us -> none  [shards(): lax.all_gather(value_weight, 'fs', axis=0, tiled=True)]
    all_gather x1, waiting for transfers between devices: 136 us -> 149 us  [shards(): lax.all_gather(up_weight, 'fs', axis=0, tiled=True)]
    all_gather x1, waiting for transfers between devices: 149 us -> 136 us  [shards(): lax.all_gather(down_turned_shard, 'fs', axis=0, tiled=True)]
  transfers between devices with their start and end apart: 7 -> 9, of which waited for: 7 -> 8; matrix products, arithmetic and copies ran while one was open for 3% -> 3% of each run, Pallas kernels for 0% -> 0%
where the time goes in v1:
time: 447 us
  waiting for transfers between devices  377 us (84%)
  blocking collectives  24 us (5%)
  matrix products  16.4 us (4%)
  between operations  13.6 us (3%)
  other arithmetic  9.99 us (2%)
    all_gather x1, waiting for transfers between devices, shards(): lax.all_gather(up_weight, 'fs', axis=0, tiled=True)  149 us
    all_gather x1, waiting for transfers between devices, shards(): lax.all_gather(down_turned_shard, 'fs', axis=0, tiled=True)  136 us
    ppermute x3, waiting for transfers between devices, _define_levels_all(): small = lax.ppermute(leaves[-1], axis_id, buffer)  35.2 us
    reduce_scatter x1, waiting for transfers between devices, shards(): lax.psum_scatter(fed_terms.astype(jnp.bfloat16), 'tp', scatter_dimension=...  20 us
    reduce_scatter x1, waiting for transfers between devices, shards(): lax.psum_scatter(partial_terms.astype(jnp.bfloat16), 'tp', scatter_dimens...  19.2 us
    all_gather x1, waiting for transfers between devices, shards(): lax.all_gather(out_turned_shard, 'fs', axis=0, tiled=True)  15.2 us
    dot_general x2, matrix products, contract(): lax.dot_general(left, turned, (((1,), (1,)), ((), ())), preferred_element...  11.3 us
  transfers between devices with their start and end apart: 9, of which 8 were waited for; matrix products, arithmetic and copies ran while one was open for 3% of the time, Pallas kernels for 0%

profile of v1, /device:TPU:0, one launch (start us, length us, event | category | flops | bytes accessed | tf_op | source)
XLA Modules:
  0.0 446.8 jit_solution(12239456970679076502)
XLA Ops:
  6.5 0.7 all-gather.5.cloned.1.call-update
  7.3 3.1 collective-permute-start
  10.5 1.2 convert_reduce_fusion
  11.7 7.3 %collective-permute-done = bf16[512,256]{1,0:T(8,128)(2,1)S(1)} collective-permute-done((bf16[512,256]{1,0:T(8,128)(2,1)}, bf16[512,256]{1,0:T(8,128)(2,1)S(1)}, u32[]{:S(2)}, u32[]{:S(2)}) %collective-permute-start) | collective-permute-done | bytes 262176 | tf_op jit(solution)/shard_map/ppermute | solution.py:62
  19.0 1.3 fusion.11
  20.3 13.8 %collective-permute-done.1 = bf16[512,256]{1,0:T(8,128)(2,1)S(1)} collective-permute-done((bf16[512,256]{1,0:T(8,128)(2,1)S(1)}, bf16[512,256]{1,0:T(8,128)(2,1)S(1)}, u32[]{:S(2)}, u32[]{:S(2)}) %collective-permute-start.1) | collective-permute-done | bytes 262176 | tf_op jit(solution)/shard_map/ppermute | solution.py:62
  34.1 1.1 collective-permute-start.2
  35.1 1.4 fusion.13
  36.6 14.2 %collective-permute-done.2 = bf16[512,256]{1,0:T(8,128)(2,1)S(1)} collective-permute-done((bf16[512,256]{1,0:T(8,128)(2,1)S(1)}, bf16[512,256]{1,0:T(8,128)(2,1)S(1)}, u32[]{:S(2)}, u32[]{:S(2)}) %collective-permute-start.2) | collective-permute-done | bytes 262176 | tf_op jit(solution)/shard_map/ppermute | solution.py:62
  50.8 1.1 pad_maximum_fusion
  51.9 0.6 gather_fusion
  52.5 1.4 fusion.18
  53.9 1.6 fusion.7
  55.5 2.2 fusion.43
  57.8 5.7 %all-reduce.2 = (f32[128]{0:T(128)S(1)}, f32[128]{0:T(128)S(1)}) all-reduce(f32[128]{0:T(128)S(1)} %fusion.30, f32[128]{0:T(128)S(1)} %get-tuple-element.21), channel_id=1, replica_groups=mesh['grp'=2,'fs'=4,'tp'=4] {'tp'}, use_global_device_ids=true, to_apply=%region_5.6 | all-reduce | flops 256 | bytes 2048 | tf_op jit(solution)/shard_map/psum | solution.py:100
  63.5 15.2 %all-gather.7.cloned.1.call-done = bf16[2048,256]{0,1:T(8,128)(2,1)} async-done(((bf16[512,256]{0,1:T(8,128)(2,1)}), bf16[2048,256]{0,1:T(8,128)(2,1)}) %all-gather.7.cloned.1.call-update) | async-done | bytes 1048592 | tf_op jit(solution)/shard_map/all_gather | solution.py:80
  78.6 2.4 convolution_convert_fusion.1
  81.1 0.5 all-gather.11.cloned.1.call-update
  81.7 0.5 all-gather.9.cloned.1.call-update
  82.3 0.8 dynamic_slice.7
  83.0 19.2 %reduce-scatter.3.cloned.1.call-done = bf16[128,512]{1,0:T(8,128)(2,1)} async-done(((bf16[128,2048]{1,0:T(8,128)(2,1)}), bf16[128,512]{1,0:T(8,128)(2,1)}) %reduce-scatter.3.cloned.1.call-update) | async-done | bytes 131088 | tf_op jit(solution)/shard_map/reduce_scatter | solution.py:105
  102.2 1.0 fusion.24
  103.3 5.8 %all-reduce.1 = (f32[128]{0:T(128)S(1)}, f32[128]{0:T(128)S(1)}) all-reduce(f32[128]{0:T(128)S(1)} %get-tuple-element.6, f32[128]{0:T(128)S(1)} %get-tuple-element.5), channel_id=1, replica_groups=mesh['grp'=2,'fs'=4,'tp'=4] {'tp'}, use_global_device_ids=true, to_apply=%region_10.11 | all-reduce | flops 256 | bytes 2048 | tf_op jit(solution)/shard_map/psum | solution.py:111
  109.0 1.0 multiply_convert_fusion.1
  110.1 6.8 %all_gather.17 = bf16[128,2048]{1,0:T(8,128)(2,1)S(1)} all-gather(bf16[128,512]{1,0:T(8,128)(2,1)S(1)} %multiply_convert_fusion.1), channel_id=1, replica_groups=mesh['grp'=2,'fs'=4,'tp'=4] {'tp'}, dimensions={1}, use_global_device_ids=true | all-gather | bytes 655360 | tf_op jit(solution)/shard_map/all_gather | solution.py:113
  116.9 136.4 %all-gather.11.cloned.1.call-done = bf16[2048,2048]{0,1:T(8,128)(2,1)} async-done(((bf16[512,2048]{0,1:T(8,128)(2,1)}), bf16[2048,2048]{0,1:T(8,128)(2,1)}) %all-gather.11.cloned.1.call-update) | async-done | bytes 8388624 | tf_op jit(solution)/shard_map/all_gather | solution.py:82
  253.3 149.3 %all-gather.9.cloned.1.call-done = bf16[2048,2048]{1,0:T(8,128)(2,1)} async-done(((bf16[512,2048]{1,0:T(8,128)(2,1)}), bf16[2048,2048]{1,0:T(8,128)(2,1)}) %all-gather.9.cloned.1.call-update) | async-done | bytes 8388624 | tf_op jit(solution)/shard_map/all_gather | solution.py:81
  402.5 8.9 %convolution_convert_fusion = bf16[128,2048]{1,0:T(8,128)(2,1)} fusion(bf16[2048,2048]{0,1:T(8,128)(2,1)} %all-gather.11.cloned.1.call-done, bf16[128,2048]{1,0:T(8,128)(2,1)S(1)} %all_gather.17, bf16[2048,2048]{1,0:T(8,128)(2,1)} %all-gather.9.cloned.1.call-done), kind=kOutput, calls=%fused_computation.3 | convolution fusion | flops 2148532224 | bytes 17825792 | tf_op jit(solution)/shard_map/dot_general | solution.py:35
  411.5 20.0 %reduce-scatter.5.cloned.1.call-done = bf16[128,512]{1,0:T(8,128)(2,1)} async-done(((bf16[128,2048]{1,0:T(8,128)(2,1)}), bf16[128,512]{1,0:T(8,128)(2,1)}) %reduce-scatter.5.cloned.1.call-update) | async-done | bytes 131088 | tf_op jit(solution)/shard_map/reduce_scatter | solution.py:118
  431.5 1.0 fusion.25
  432.5 5.8 %all-reduce = (f32[128]{0:T(128)S(1)}, f32[128]{0:T(128)S(1)}) all-reduce(f32[128]{0:T(128)S(1)} %get-tuple-element.8, f32[128]{0:T(128)S(1)} %get-tuple-element.7), channel_id=1, replica_groups=mesh['grp'=2,'fs'=4,'tp'=4] {'tp'}, use_global_device_ids=true, to_apply=%region_15.16 | all-reduce | flops 256 | bytes 2048 | tf_op jit(solution)/shard_map/psum | solution.py:120
  438.3 1.7 fusion.26
  (27 shorter events, 0.5 us)
Async XLA Ops:
  6.5 49.0 %copy-start = (bf16[31,256]{1,0:T(8,128)(2,1)S(1)}, bf16[31,256]{1,0:T(8,128)(2,1)}, u32[]{:S(2)}) copy-start(bf16[31,256]{1,0:T(8,128)(2,1)} %param.16) | copy-start | bytes 47620
  6.5 72.1 %copy-start.3 = (f32[256]{0:T(256)S(1)}, f32[256]{0:T(256)}, u32[]{:S(2)}) copy-start(f32[256]{0:T(256)} %param.17) | copy-start | bytes 3076
  6.5 72.1 %copy-start.2 = (f32[256]{0:T(256)S(1)}, f32[256]{0:T(256)}, u32[]{:S(2)}) copy-start(f32[256]{0:T(256)} %param.18) | copy-start | bytes 3076
  6.5 47.4 %all-gather.5.cloned.1.call-start = ((), (), s32[]{:S(2)}) async-start(), calls=%async_computation.2 | async-start | bytes 1310720 | tf_op jit(solution)/shard_map/all_gather | solution.py:79
  7.3 71.4 %all-gather.7.cloned.1.call-start = ((), (), s32[]{:S(2)}) async-start(), calls=%async_computation.3 | async-start | bytes 1310720 | tf_op jit(solution)/shard_map/all_gather | solution.py:80
  7.3 11.6 %collective-permute-start = (bf16[512,256]{1,0:T(8,128)(2,1)}, bf16[512,256]{1,0:T(8,128)(2,1)S(1)}, u32[]{:S(2)}, u32[]{:S(2)}) collective-permute-start(bf16[512,256]{1,0:T(8,128)(2,1)} %param.14), channel_id=1, source_target_pairs={{0,4},{4,8},{8,12},{12,0},{1,5},{5,9},{9,13},{13,1},{2,6},{6,10},{... | collective-permute-start | bytes 786440 | tf_op jit(solution)/shard_map/ppermute | solution.py:62
  10.4 91.8 %reduce-scatter.3.cloned.1.call-start = ((), (), s32[]{:S(2)}) async-start(), calls=%async_computation.4 | async-start | bytes 655360 | tf_op jit(solution)/shard_map/reduce_scatter | solution.py:105
  19.0 15.1 %collective-permute-start.1 = (bf16[512,256]{1,0:T(8,128)(2,1)S(1)}, bf16[512,256]{1,0:T(8,128)(2,1)S(1)}, u32[]{:S(2)}, u32[]{:S(2)}) collective-permute-start(bf16[512,256]{1,0:T(8,128)(2,1)S(1)} %collective-permute-done), channel_id=1, source_target_pairs={{0,4},{4,8},{8,12},{12,0},{1,5},{5,9},{9,13},{13,1},{2,6},{6,10},{... | collective-permute-start | bytes 786440 | tf_op jit(solution)/shard_map/ppermute | solution.py:62
  34.1 16.7 %collective-permute-start.2 = (bf16[512,256]{1,0:T(8,128)(2,1)S(1)}, bf16[512,256]{1,0:T(8,128)(2,1)S(1)}, u32[]{:S(2)}, u32[]{:S(2)}) collective-permute-start(bf16[512,256]{1,0:T(8,128)(2,1)S(1)} %collective-permute-done.1), channel_id=1, source_target_pairs={{0,4},{4,8},{8,12},{12,0},{1,5},{5,9},{9,13},{13,1},{2,6},{6,10},{... | collective-permute-start | bytes 786440 | tf_op jit(solution)/shard_map/ppermute | solution.py:62
  81.0 172.2 %all-gather.11.cloned.1.call-start = ((), (), s32[]{:S(2)}) async-start(), calls=%async_computation.6 | async-start | bytes 10485760 | tf_op jit(solution)/shard_map/all_gather | solution.py:82
  81.6 320.9 %all-gather.9.cloned.1.call-start = ((), (), s32[]{:S(2)}) async-start(), calls=%async_computation.5 | async-start | bytes 10485760 | tf_op jit(solution)/shard_map/all_gather | solution.py:81
  82.2 349.3 %reduce-scatter.5.cloned.1.call-start = ((), (), s32[]{:S(2)}) async-start(), calls=%async_computation.7 | async-start | bytes 655360 | tf_op jit(solution)/shard_map/reduce_scatter | solution.py:118
  116.9 321.4 %copy-start.1 = (f32[512]{0:T(512)S(1)}, f32[512]{0:T(512)}, u32[]{:S(2)}) copy-start(f32[512]{0:T(512)} %param.23) | copy-start | bytes 6148
Sparse Core Ops, SparseCore 0:
  8.9 41.9 all-gather.4
  52.4 26.1 all-gather.6
  81.2 20.9 reduce-scatter.2
  103.6 149.5 all-gather.10
  254.7 147.7 all-gather.8
  411.6 19.8 reduce-scatter.4
